TPU v7x, 32 devices: a whole 2x2x4 slice. The times are simulated.
32 devices in a mesh: ep: 8 (over z, x), tp: 4 (over y, core).
Axes of the slice: x: 2, y: 2, z: 4, core: 2. Of those that a mesh axis runs over, the one named last changes fastest.
Arguments:
- hidden: bfloat16 [32, 2048], P('ep'), may hold values from -6 to 6
- attn_gain: float32 [2048], replicated, may hold values from 0.3 to 3
- query_weight: bfloat16 [2048, 2048], P('ep', 'tp'), may hold values from -0.125 to 0.125
- head_bias: float32 [16], replicated, may hold values from -10 to -4
- key_cache: bfloat16 [32, 4, 1024, 128], P('ep', 'tp'), may hold values from -6 to 6
- value_cache: bfloat16 [32, 4, 1024, 128], P('ep', 'tp'), may hold values from -7 to 7
- lengths: int32 [32], P('ep'), may hold values from 256 to 1024, as said below
- out_weight: bfloat16 [2048, 2048], P('tp', 'ep'), may hold values from -0.125 to 0.125
- moe_gain: float32 [2048], replicated, may hold values from 0.1 to 1.9
- route_group: int32 [32], P('ep'), may hold values from 0 to 1, as said below
- route_inner: int32 [32, 2], P('ep'), may hold values from 0 to 3, as said below
- route_weight: bfloat16 [32, 2], P('ep'), may hold values from 0.25 to 1
- gate_w: bfloat16 [8, 2048, 768], P('ep', None, 'tp'), may hold values from -0.125 to 0.125
- up_w: bfloat16 [8, 2048, 768], P('ep', None, 'tp'), may hold values from -0.125 to 0.125
- down_w: bfloat16 [8, 768, 2048], P('ep', 'tp'), may hold values from -0.21875 to 0.21875
Outputs:
- mixed: bfloat16 [32, 2048], P('ep', 'tp')
Inputs may be any that keep to these rules, and one draw needn't show every extreme that they name: `lengths`: some sequence has length 1024 in every draw. Within the rows of one device (aligned blocks of 4 rows) no expert route_group * 4 + route_inner is named twice; one expert is named in every block. `route_inner`: the 2 entries of a row differ.
All inputs are finite; a program needn't handle non-finite values.
Results may differ from a plain program's by a relative error of at most 0.013.
Values may be sent and summed in bfloat16 or wider, within the bound.
A program may use at most 64 MiB of HBM per device.

v0:
```python
import jax
import jax.numpy as jnp
from jax import lax
from jax.sharding import PartitionSpec as P

rms_epsilon = 1e-06


def rms_scale(values, gain):
    wide = values.astype(jnp.float32)
    scaled = wide * lax.rsqrt(jnp.mean(wide * wide, axis=-1, keepdims=True) + rms_epsilon)
    return (scaled * gain).astype(jnp.bfloat16)


def body(
    hidden,
    attn_gain,
    query_weight,
    head_bias,
    key_cache,
    value_cache,
    lengths,
    out_weight,
    moe_gain,
    route_group,
    route_inner,
    route_weight,
    gate_w,
    up_w,
    down_w,
):
    n_tp = lax.axis_size("tp")
    n_ep = lax.axis_size("ep")
    tokens = hidden.shape[0]
    d_model = hidden.shape[1]
    normed = rms_scale(hidden, attn_gain)
    feature_block = lax.all_to_all(normed, "ep", split_axis=1, concat_axis=0, tiled=True)
    queries = lax.psum_scatter(
        jnp.dot(feature_block, query_weight, preferred_element_type=jnp.float32),
        "ep",
        scatter_dimension=0,
        tiled=True,
    ).astype(jnp.bfloat16)
    head_size = key_cache.shape[3]
    local_kv = key_cache.shape[1]
    cache_len = key_cache.shape[2]
    local_heads = queries.shape[1] // head_size
    group_heads = local_heads // local_kv
    queries = queries.reshape(tokens, local_kv, group_heads, head_size)
    own_bias = lax.dynamic_slice_in_dim(
        head_bias, lax.axis_index("tp") * local_heads, local_heads, 0
    )
    own_bias = own_bias.reshape(local_kv, group_heads)
    scores = jnp.einsum(
        "tkgd,tkpd->tkgp", queries, key_cache, preferred_element_type=jnp.float32
    ) * head_size ** (-0.5)
    scores = scores + own_bias[None, :, :, None]
    position = jnp.arange(cache_len, dtype=jnp.int32)
    visible = position[None, None, None, :] < lengths[:, None, None, None]
    log_keep = jnp.where(visible, jax.nn.log_sigmoid(-scores), 0.0)
    later_sum = lax.cumsum(log_keep, axis=3, reverse=True) - log_keep
    weight = jnp.where(visible, jnp.exp(jax.nn.log_sigmoid(scores) + later_sum), 0.0).astype(
        jnp.bfloat16
    )
    heads_out = jnp.einsum(
        "tkgp,tkpd->tkgd", weight, value_cache, preferred_element_type=jnp.float32
    )
    heads_out = heads_out.astype(jnp.bfloat16).reshape(tokens, -1)
    partial_value = jnp.dot(
        heads_out,
        lax.all_gather(out_weight, "ep", axis=1, tiled=True),
        preferred_element_type=jnp.float32,
    )
    rounded = lax.optimization_barrier(partial_value.astype(jnp.bfloat16)).astype(jnp.float32)
    attended = lax.psum(rounded.astype(jnp.bfloat16), "tp").astype(jnp.float32)
    residual = (hidden.astype(jnp.float32) + attended).astype(jnp.bfloat16)
    normed_two = rms_scale(residual, moe_gain)
    per_device = gate_w.shape[0]
    experts = per_device * n_ep
    group_count = max(2, experts // 32)
    group_size = experts // group_count
    chosen = route_group[:, None] * group_size + route_inner
    matches = chosen[:, :, None] == jnp.arange(experts, dtype=jnp.int32)[None, None, :]
    picked = jnp.any(matches, axis=1).astype(jnp.bfloat16)
    mixing = jnp.sum(
        jnp.where(matches, route_weight[:, :, None].astype(jnp.float32), 0.0), axis=1
    ).astype(jnp.bfloat16)
    part_width = d_model // n_tp
    outgoing = jnp.einsum("te,td->ed", picked, normed_two, preferred_element_type=jnp.float32)
    outgoing = outgoing.astype(jnp.bfloat16).reshape(n_ep, per_device, d_model)
    arrived = lax.all_to_all(outgoing, "ep", split_axis=0, concat_axis=0, tiled=True)
    gated_in = jnp.einsum("sed,edf->sef", arrived, gate_w, preferred_element_type=jnp.float32)
    up_proj = jnp.einsum("sed,edf->sef", arrived, up_w, preferred_element_type=jnp.float32)
    activated = (jax.nn.silu(gated_in) * up_proj).astype(jnp.bfloat16)
    down_out = jnp.einsum("sef,efd->sed", activated, down_w, preferred_element_type=jnp.float32)
    down_rounded = lax.optimization_barrier(down_out.astype(jnp.bfloat16)).astype(jnp.float32)
    summed = lax.psum_scatter(
        down_rounded.astype(jnp.bfloat16), "tp", scatter_dimension=2, tiled=True
    )
    returned = lax.all_to_all(summed, "ep", split_axis=0, concat_axis=0, tiled=True).reshape(
        experts, part_width
    )
    routed = jnp.dot(mixing, returned, preferred_element_type=jnp.float32)
    own_residual = lax.dynamic_slice_in_dim(
        residual, lax.axis_index("tp") * part_width, part_width, 1
    )
    return (own_residual.astype(jnp.float32) + routed).astype(jnp.bfloat16)


def solution(mesh):
    placed = (
        P("ep", None),
        P(),
        P("ep", "tp"),
        P(),
        P("ep", "tp", None, None),
        P("ep", "tp", None, None),
        P("ep"),
        P("tp", "ep"),
        P(),
        P("ep"),
        P("ep", None),
        P("ep", None),
        P("ep", None, "tp"),
        P("ep", None, "tp"),
        P("ep", "tp", None),
    )
    return jax.shard_map(body, mesh=mesh, in_specs=placed, out_specs=P("ep", "tp"), check_vma=False)
```

profile of v0, /device:TPU:0, one launch (start us, length us, event | category | flops | bytes accessed | tf_op | source)
XLA Modules:
  0.0 150.5 jit_solution(8893848438040312585)
XLA Ops:
  6.5 0.0 copy-start
  6.5 0.0 all-gather.2.cloned.1.call-start
  6.5 0.7 all-gather.2.cloned.1.call-update
  7.3 0.8 fusion.25
  8.1 1.4 fusion.27
  9.5 7.3 %all-to-all-start = ((bf16[4,8,256]{2,0,1:T(4,128)(2,1)}), bf16[4,8,256]{2,0,1:T(4,128)(2,1)S(1)}, u32[]{:S(2)}, u32[]{:S(2)}) async-start(bf16[4,8,256]{2,0,1:T(4,128)(2,1)} %bitcast), calls=%async_computation | async-start | bytes 32768 | tf_op jit(solution)/shard_map/all_to_all | solution.py:37
  16.8 0.0 reduce-scatter.2.cloned.1.call-start
  16.8 0.7 broadcast_multiply_fusion
  17.5 0.7 broadcast_add_fusion
  18.2 0.0 copy-start.6
  18.2 0.7 iota_compare_fusion
  18.9 0.0 copy-start.5
  18.9 0.6 fusion.51
  19.5 0.7 dynamic_slice.6
  20.2 1.3 dynamic-slice
  22.1 1.4 all-to-all-done
  23.5 0.0 copy-done.6
  23.5 1.1 fusion.57
  24.6 37.7 %all-reduce = bf16[32,512]{1,0:T(8,128)(2,1)S(1)} all-reduce(f32[32,512]{1,0:T(8,128)S(1)} %fusion.57), channel_id=2, replica_groups=mesh['ep'=8,'tp'=4] {'ep'}, use_global_device_ids=true, to_apply=%region_1.0.clone | all-reduce | flops 16384 | bytes 98304
  62.3 0.0 copy-done
  62.3 0.4 fusion.21
  62.7 0.0 copy-done.5
  62.8 0.0 copy-start.4
  62.8 19.8 %reduce-window.6 = f32[4,1,4,8,128]{4,3,2,1,0:T(8,128)S(1)} reduce-window(f32[4,1,4,8,128]{4,3,2,1,0:T(8,128)S(1)} %bitcast.82, f32[]{:T(128)} %constant.12.clone.1), window={size=1x1x1x1x128 pad=0_0x0_0x0_0x0_0x0_127}, to_apply=%region_2.3 | reduce-window | flops 2080768 | bytes 131076 | tf_op jit(solution)/shard_map/reduce-window
  82.6 0.1 slice_reduce_fusion
  82.7 0.7 reduce-window.9
  83.4 0.1 slice_bitcast_fusion
  83.5 0.0 copy-start.1
  83.5 0.1 broadcast.72
  83.6 0.7 reshape.151
  84.3 0.0 copy-start.2
  84.3 0.0 copy-start.3
  84.3 2.4 %fusion.6 = bf16[1,4,4,128]{3,2,1,0:T(4,128)(2,1)} fusion(bf16[4,1,1024,128]{3,2,1,0:T(8,128)(2,1)} %param.20, f32[4,4,1024]{2,1,0:T(4,128)S(1)} %reshape.148, f32[4,4,1024]{2,1,0:T(4,128)} %reshape.151, f32[4,4,1024]{2,1,0:T(4,128)S(1)} %get-tuple-element.8, pred[4,1024]{1,0:T(4,128)(4,1)} %copy-done.5), kind=kOutput, calls=%fused_computation.14 | convolution fusion | flops 4540416 | bytes 1253376 | tf_op jit(solution)/shard_map/tkgp,tkpd->tkgd/dot_general | solution.py:65
  86.6 0.0 copy-start.8
  86.6 0.0 copy-start.7
  86.6 0.0 all-gather.2.cloned.1.call-done
  86.6 2.0 %convolution_convert_fusion.2 = bf16[4,2048]{1,0:T(4,128)(2,1)S(1)} fusion(bf16[512,2048]{1,0:T(8,128)(2,1)} %all-gather.2.cloned.1.call-done, bf16[1,4,4,128]{3,2,1,0:T(4,128)(2,1)} %fusion.6), kind=kOutput, calls=%fused_computation.4 | convolution fusion | flops 8396800 | bytes 2117632 | tf_op jit(solution)/shard_map/dot_general | solution.py:69
  88.6 10.1 %psum.7 = bf16[4,2048]{1,0:T(4,128)(2,1)S(1)} all-reduce(bf16[4,2048]{1,0:T(4,128)(2,1)S(1)} %convolution_convert_fusion.2), channel_id=1, replica_groups=mesh['ep'=8,'tp'=4] {'tp'}, use_global_device_ids=true, to_apply=%region_4.5 | all-reduce | flops 8192 | bytes 32768 | tf_op jit(solution)/shard_map/psum | solution.py:75
  98.7 0.0 copy-done.4
  98.7 0.1 fusion.22
  98.9 0.9 fusion
  99.8 0.5 broadcast.80
  100.3 0.7 reduce.2
  101.0 9.1 %all_to_all.29 = bf16[8,2,1024]{2,1,0:T(2,128)(2,1)S(1)} all-to-all(bf16[8,2,1024]{2,1,0:T(2,128)(2,1)S(1)} %reshape.163), channel_id=1, replica_groups=mesh['ep'=8,'tp'=4] {'ep'}, dimensions={0} | all-to-all | bytes 65536 | tf_op jit(solution)/shard_map/all_to_all | solution.py:91
  110.1 0.0 copy-done.1
  110.1 0.3 convolution_bitcast_fusion.1
  110.4 0.0 copy-done.2
  110.4 0.0 copy-done.3
  110.4 1.3 fusion.1
  111.7 0.0 reduce-scatter.2.cloned.1.call-update
  111.7 0.0 copy-done.8
  111.8 17.1 %reduce-scatter.2.cloned.1.call-done = bf16[8,1,512]{2,0,1:T(8,128)(2,1)} async-done(((bf16[8,1,2048]{2,0,1:T(8,128)(2,1)}), bf16[8,1,512]{2,0,1:T(8,128)(2,1)}) %reduce-scatter.2.cloned.1.call-update) | async-done | bytes 8208 | tf_op jit(solution)/shard_map/reduce_scatter | solution.py:97
  128.9 1.3 reduce.3
  130.2 0.6 reshape.165
  130.9 5.5 %all-to-all-start.2 = ((bf16[8,2,256]{2,1,0:T(2,128)(2,1)}), bf16[8,2,256]{2,1,0:T(2,128)(2,1)S(1)}, u32[]{:S(2)}, u32[]{:S(2)}) async-start(bf16[8,2,256]{2,1,0:T(2,128)(2,1)} %reshape.165), calls=%async_computation.3 | async-start | bytes 16384 | tf_op jit(solution)/shard_map/all_to_all | solution.py:100
  136.4 0.0 copy-done.7
  136.4 0.1 select_reduce_fusion
  136.5 6.4 %all-to-all-done.2 = bf16[8,2,256]{2,1,0:T(2,128)(2,1)S(1)} async-done(((bf16[8,2,256]{2,1,0:T(2,128)(2,1)}), bf16[8,2,256]{2,1,0:T(2,128)(2,1)S(1)}, u32[]{:S(2)}, u32[]{:S(2)}) %all-to-all-start.2) | async-done | bytes 8224 | tf_op jit(solution)/shard_map/all_to_all | solution.py:100
  142.9 0.7 fusion.4
  (11 shorter events, 0.2 us)
Async XLA Ops:
  6.5 55.8 %copy-start = (bf16[4,1,1024,128]{3,2,1,0:T(8,128)(2,1)S(1)}, bf16[4,1,1024,128]{3,2,1,0:T(8,128)(2,1)}, u32[]{:S(2)}) copy-start(bf16[4,1,1024,128]{3,2,1,0:T(8,128)(2,1)} %param.19) | copy-start | bytes 3145732
  6.5 80.1 %all-gather.2.cloned.1.call-start = ((), (), s32[]{:S(2)}) async-start(), calls=%async_computation.4 | async-start | bytes 2359296 | tf_op jit(solution)/shard_map/all_gather | solution.py:71
  9.5 14.0 %all-to-all-start = ((bf16[4,8,256]{2,0,1:T(4,128)(2,1)}), bf16[4,8,256]{2,0,1:T(4,128)(2,1)S(1)}, u32[]{:S(2)}, u32[]{:S(2)}) async-start(bf16[4,8,256]{2,0,1:T(4,128)(2,1)} %bitcast), calls=%async_computation | async-start | bytes 32768 | tf_op jit(solution)/shard_map/all_to_all | solution.py:37
  16.8 112.1 %reduce-scatter.2.cloned.1.call-start = ((), (), s32[]{:S(2)}) async-start(), calls=%async_computation.5 | async-start | bytes 40960 | tf_op jit(solution)/shard_map/reduce_scatter | solution.py:97
  18.2 5.3 %copy-start.6 = (s32[4,2]{0,1:T(2,128)}, s32[4,2]{0,1:T(2,128)S(1)}, u32[]{:S(2)}) copy-start(s32[4,2]{0,1:T(2,128)S(1)} %broadcast_add_fusion) | copy-start | bytes 100
  18.9 43.8 %copy-start.5 = (pred[4,1024]{1,0:T(4,128)(4,1)}, pred[4,1024]{1,0:T(4,128)(4,1)S(1)}, u32[]{:S(2)}) copy-start(pred[4,1024]{1,0:T(4,128)(4,1)S(1)} %iota_compare_fusion) | copy-start | bytes 12292
  62.8 36.0 %copy-start.4 = (bf16[4,2048]{1,0:T(4,128)(2,1)S(1)}, bf16[4,2048]{1,0:T(4,128)(2,1)}, u32[]{:S(2)}) copy-start(bf16[4,2048]{1,0:T(4,128)(2,1)} %param.15) | copy-start | bytes 49156
  83.5 26.6 %copy-start.1 = (bf16[1,2048,192]{1,2,0:T(8,128)(2,1)S(1)}, bf16[1,2048,192]{1,2,0:T(8,128)(2,1)}, u32[]{:S(2)}) copy-start(bf16[1,2048,192]{1,2,0:T(8,128)(2,1)} %param.27) | copy-start | bytes 2359300
  84.3 26.2 %copy-start.2 = (bf16[1,192,2048]{2,1,0:T(8,128)(2,1)S(1)}, bf16[1,192,2048]{2,1,0:T(8,128)(2,1)}, u32[]{:S(2)}) copy-start(bf16[1,192,2048]{2,1,0:T(8,128)(2,1)} %param.29) | copy-start | bytes 2359300
  84.3 26.2 %copy-start.3 = (bf16[1,2048,192]{1,2,0:T(8,128)(2,1)S(1)}, bf16[1,2048,192]{1,2,0:T(8,128)(2,1)}, u32[]{:S(2)}) copy-start(bf16[1,2048,192]{1,2,0:T(8,128)(2,1)} %param.28) | copy-start | bytes 2359300
  86.6 25.1 %copy-start.8 = (bf16[4,2]{0,1:T(2,128)(2,1)S(1)}, bf16[4,2]{0,1:T(2,128)(2,1)}, u32[]{:S(2)}) copy-start(bf16[4,2]{0,1:T(2,128)(2,1)} %param.26) | copy-start | bytes 52
  86.6 49.8 %copy-start.7 = (s32[4,2]{0,1:T(2,128)S(1)}, s32[4,2]{0,1:T(2,128)}, u32[]{:S(2)}) copy-start(s32[4,2]{0,1:T(2,128)} %copy-done.6) | copy-start | bytes 100
  130.9 12.0 %all-to-all-start.2 = ((bf16[8,2,256]{2,1,0:T(2,128)(2,1)}), bf16[8,2,256]{2,1,0:T(2,128)(2,1)S(1)}, u32[]{:S(2)}, u32[]{:S(2)}) async-start(bf16[8,2,256]{2,1,0:T(2,128)(2,1)} %reshape.165), calls=%async_computation.3 | async-start | bytes 16384 | tf_op jit(solution)/shard_map/all_to_all | solution.py:100
Sparse Core Ops, SparseCore 0:
  9.4 54.2 all-gather.1
  111.9 16.9 reduce-scatter.1
where the time goes:
time: 151 us; the launch traced here: 150 us
  blocking collectives  56.9 us (38%)
  other arithmetic  27.7 us (18%)
  waiting for transfers between devices  25.6 us (17%)
  between operations  14.1 us (9%)
  starting transfers between devices  12.8 us (8%)
  matrix products  9.09 us (6%)
  local copies, waits for them, and re-layouts  4.21 us (3%)
    unnamed x1, blocking collectives  37.7 us
    another operation x2, other arithmetic  20.5 us
    reduce_scatter x1, waiting for transfers between devices, body(): lax.psum_scatter(down_rounded.astype(jnp.bfloat16), 'tp', scatter_dimensi...  17.1 us
    psum x1, blocking collectives, body(): attended = lax.psum(rounded.astype(jnp.bfloat16), 'tp').astype(jnp.float32)  10.1 us
    all_to_all x1, blocking collectives, body(): lax.all_to_all(outgoing, 'ep', split_axis=0, concat_axis=0, tiled=True)  9.06 us
    all_to_all x1, starting transfers between devices, body(): lax.all_to_all(normed, 'ep', split_axis=1, concat_axis=0, tiled=True)  7.28 us
    all_to_all x1, waiting for transfers between devices, body(): lax.all_to_all(summed, 'ep', split_axis=0, concat_axis=0, tiled=True)  6.43 us
    all_to_all x1, starting transfers between devices, body(): lax.all_to_all(summed, 'ep', split_axis=0, concat_axis=0, tiled=True)  5.51 us
  transfers between devices with their start and end apart: 4, of which 3 were waited for; matrix products, arithmetic and copies ran while one was open for 22% of the time, Pallas kernels for 0%

commit v1 on v0

--- a/solution.py
+++ b/solution.py
@@ -72,7 +72,9 @@
         preferred_element_type=jnp.float32,
     )
     rounded = lax.optimization_barrier(partial_value.astype(jnp.bfloat16)).astype(jnp.float32)
-    attended = lax.psum(rounded.astype(jnp.bfloat16), "tp").astype(jnp.float32)
+    attended = jnp.sum(lax.all_gather(rounded.astype(jnp.bfloat16), "tp"), axis=0).astype(
+        jnp.float32
+    )
     residual = (hidden.astype(jnp.float32) + attended).astype(jnp.bfloat16)
     normed_two = rms_scale(residual, moe_gain)
     per_device = gate_w.shape[0]

time: 151 us -> 143 us (0.947)
  blocking collectives: 56.9 us -> 51.5 us
  matrix products: 9.09 us -> 6.49 us
    psum x1 -> x0, blocking collectives: 10.1 us -> none  [body(): attended = lax.psum(rounded.astype(jnp.bfloat16), 'tp').astype(jnp.float32)]
    all_gather x0 -> x1, blocking collectives: none -> 5.23 us  [body(): lax.all_gather(rounded.astype(jnp.bfloat16), 'tp')]
    dot_general x1, matrix products: 2.35 us -> 0.36 us  [body(): jnp.einsum('tkgp,tkpd->tkgd', weight, value_cache, preferred_element_type...]
  transfers between devices with their start and end apart: 4 -> 4, of which waited for: 3 -> 3; matrix products, arithmetic and copies ran while one was open for 22% -> 21% of each run, Pallas kernels for 0% -> 0%
where the time goes in v1:
time: 143 us; the launch traced here: 142 us
  blocking collectives  51.5 us (36%)
  other arithmetic  27.2 us (19%)
  waiting for transfers between devices  26 us (18%)
  between operations  14.2 us (10%)
  starting transfers between devices  12.8 us (9%)
  matrix products  6.49 us (5%)
  local copies, waits for them, and re-layouts  3.55 us (2%)
    unnamed x1, blocking collectives  37.2 us
    another operation x2, other arithmetic  20.5 us
    reduce_scatter x1, waiting for transfers between devices, body(): lax.psum_scatter(down_rounded.astype(jnp.bfloat16), 'tp', scatter_dimensi...  17 us
    all_to_all x1, blocking collectives, body(): lax.all_to_all(outgoing, 'ep', split_axis=0, concat_axis=0, tiled=True)  9.06 us
    all_to_all x1, starting transfers between devices, body(): lax.all_to_all(normed, 'ep', split_axis=1, concat_axis=0, tiled=True)  7.28 us
    all_to_all x1, waiting for transfers between devices, body(): lax.all_to_all(summed, 'ep', split_axis=0, concat_axis=0, tiled=True)  6.44 us
    all_to_all x1, starting transfers between devices, body(): lax.all_to_all(summed, 'ep', split_axis=0, concat_axis=0, tiled=True)  5.51 us
    all_gather x1, blocking collectives, body(): lax.all_gather(rounded.astype(jnp.bfloat16), 'tp')  5.23 us
  transfers between devices with their start and end apart: 4, of which 3 were waited for; matrix products, arithmetic and copies ran while one was open for 21% of the time, Pallas kernels for 0%

profile of v1, /device:TPU:0, one launch (start us, length us, event | category | flops | bytes accessed | tf_op | source)
XLA Modules:
  0.0 141.9 jit_solution(7151724625158090439)
XLA Ops:
  6.5 0.0 copy-start
  6.5 0.0 copy-start.5
  6.5 0.0 all-gather.4.cloned.1.call-start
  6.5 0.7 all-gather.4.cloned.1.call-update
  7.3 0.8 fusion.25
  8.1 1.4 fusion.27
  9.5 7.3 %all-to-all-start = ((bf16[4,8,256]{2,0,1:T(4,128)(2,1)}), bf16[4,8,256]{2,0,1:T(4,128)(2,1)S(1)}, u32[]{:S(2)}, u32[]{:S(2)}) async-start(bf16[4,8,256]{2,0,1:T(4,128)(2,1)} %bitcast), calls=%async_computation | async-start | bytes 32768 | tf_op jit(solution)/shard_map/all_to_all | solution.py:37
  16.8 0.0 reduce-scatter.2.cloned.1.call-start
  16.8 0.7 broadcast_multiply_fusion
  17.5 0.7 broadcast_add_fusion
  18.2 0.7 iota_compare_fusion
  18.9 0.1 fusion.51
  19.0 0.7 dynamic_slice.6
  19.7 1.2 dynamic-slice
  21.6 1.9 %all-to-all-done = bf16[4,8,256]{2,0,1:T(4,128)(2,1)S(1)} async-done(((bf16[4,8,256]{2,0,1:T(4,128)(2,1)}), bf16[4,8,256]{2,0,1:T(4,128)(2,1)S(1)}, u32[]{:S(2)}, u32[]{:S(2)}) %all-to-all-start) | async-done | bytes 16416 | tf_op jit(solution)/shard_map/all_to_all | solution.py:37
  23.5 1.1 fusion.57
  24.6 37.2 %all-reduce = bf16[32,512]{1,0:T(8,128)(2,1)S(1)} all-reduce(f32[32,512]{1,0:T(8,128)S(1)} %fusion.57), channel_id=3, replica_groups=mesh['ep'=8,'tp'=4] {'ep'}, use_global_device_ids=true, to_apply=%region_1.0.clone | all-reduce | flops 16384 | bytes 98304
  61.8 0.0 copy-done
  61.9 0.4 fusion.21
  62.3 19.8 %reduce-window.6 = f32[4,1,4,8,128]{4,3,2,1,0:T(8,128)S(1)} reduce-window(f32[4,1,4,8,128]{4,3,2,1,0:T(8,128)S(1)} %bitcast.83, f32[]{:T(128)} %constant.13.clone.1), window={size=1x1x1x1x128 pad=0_0x0_0x0_0x0_0x0_127}, to_apply=%region_2.3 | reduce-window | flops 2080768 | bytes 131076 | tf_op jit(solution)/shard_map/reduce-window
  82.1 0.0 copy-start.4
  82.1 0.0 copy-start.6
  82.2 0.1 slice_reduce_fusion
  82.3 0.7 reduce-window.9
  83.0 0.1 slice_bitcast_fusion
  83.1 0.1 broadcast.72
  83.2 0.0 copy-start.1
  83.2 0.0 copy-done.5
  83.2 0.4 fusion.6
  83.6 0.0 copy-start.2
  83.6 0.0 copy-start.3
  83.6 0.0 copy-start.7
  83.6 0.0 all-gather.4.cloned.1.call-done
  83.6 2.1 %convolution_convert_fusion.2 = bf16[4,2048]{1,0:T(4,128)(2,1)S(1)} fusion(bf16[512,2048]{1,0:T(8,128)(2,1)} %all-gather.4.cloned.1.call-done, bf16[1,4,4,128]{3,2,1,0:T(4,128)(2,1)S(1)} %fusion.6), kind=kOutput, calls=%fused_computation.4 | convolution fusion | flops 8396800 | bytes 2117632 | tf_op jit(solution)/shard_map/dot_general | solution.py:69
  85.7 5.2 %all-gather.1 = bf16[4,4,2048]{2,1,0:T(4,128)(2,1)S(1)} all-gather(bf16[1,4,2048]{2,1,0:T(4,128)(2,1)S(1)} %bitcast.84), channel_id=2, replica_groups=mesh['ep'=8,'tp'=4] {'tp'}, dimensions={0}, use_global_device_ids=true | all-gather | bytes 81920 | tf_op jit(solution)/shard_map/all_gather | solution.py:75
  91.0 0.0 copy-done.4
  91.0 0.1 fusion.22
  91.1 0.0 copy-done.6
  91.1 0.2 fusion
  91.3 0.5 broadcast.80
  91.9 0.7 reduce.4
  92.5 9.1 %all_to_all.29 = bf16[8,2,1024]{2,1,0:T(2,128)(2,1)S(1)} all-to-all(bf16[8,2,1024]{2,1,0:T(2,128)(2,1)S(1)} %reshape.167), channel_id=1, replica_groups=mesh['ep'=8,'tp'=4] {'ep'}, dimensions={0} | all-to-all | bytes 65536 | tf_op jit(solution)/shard_map/all_to_all | solution.py:93
  101.6 0.0 copy-done.1
  101.7 0.3 convolution_bitcast_fusion.1
  102.0 0.0 copy-done.2
  102.0 0.0 copy-done.3
  102.0 1.3 fusion.1
  103.3 0.0 reduce-scatter.2.cloned.1.call-update
  103.3 0.0 copy-done.7
  103.3 17.0 %reduce-scatter.2.cloned.1.call-done = bf16[8,1,512]{2,0,1:T(8,128)(2,1)} async-done(((bf16[8,1,2048]{2,0,1:T(8,128)(2,1)}), bf16[8,1,512]{2,0,1:T(8,128)(2,1)}) %reduce-scatter.2.cloned.1.call-update) | async-done | bytes 8208 | tf_op jit(solution)/shard_map/reduce_scatter | solution.py:99
  120.3 1.3 reduce.5
  121.7 0.6 reshape.169
  122.3 5.5 %all-to-all-start.2 = ((bf16[8,2,256]{2,1,0:T(2,128)(2,1)}), bf16[8,2,256]{2,1,0:T(2,128)(2,1)S(1)}, u32[]{:S(2)}, u32[]{:S(2)}) async-start(bf16[8,2,256]{2,1,0:T(2,128)(2,1)} %reshape.169), calls=%async_computation.3 | async-start | bytes 16384 | tf_op jit(solution)/shard_map/all_to_all | solution.py:102
  127.8 0.1 select_reduce_fusion
  127.9 6.4 %all-to-all-done.2 = bf16[8,2,256]{2,1,0:T(2,128)(2,1)S(1)} async-done(((bf16[8,2,256]{2,1,0:T(2,128)(2,1)}), bf16[8,2,256]{2,1,0:T(2,128)(2,1)S(1)}, u32[]{:S(2)}, u32[]{:S(2)}) %all-to-all-start.2) | async-done | bytes 8224 | tf_op jit(solution)/shard_map/all_to_all | solution.py:102
  134.3 0.7 fusion.4
  (13 shorter events, 0.2 us)
Async XLA Ops:
  6.5 55.3 %copy-start = (bf16[4,1,1024,128]{3,2,1,0:T(8,128)(2,1)S(1)}, bf16[4,1,1024,128]{3,2,1,0:T(8,128)(2,1)}, u32[]{:S(2)}) copy-start(bf16[4,1,1024,128]{3,2,1,0:T(8,128)(2,1)} %param.19) | copy-start | bytes 3145732
  6.5 76.7 %copy-start.5 = (bf16[4,1,1024,128]{3,2,1,0:T(8,128)(2,1)S(1)}, bf16[4,1,1024,128]{3,2,1,0:T(8,128)(2,1)}, u32[]{:S(2)}) copy-start(bf16[4,1,1024,128]{3,2,1,0:T(8,128)(2,1)} %param.20) | copy-start | bytes 3145732
  6.5 77.1 %all-gather.4.cloned.1.call-start = ((), (), s32[]{:S(2)}) async-start(), calls=%async_computation.4 | async-start | bytes 2359296 | tf_op jit(solution)/shard_map/all_gather | solution.py:71
  9.5 14.0 %all-to-all-start = ((bf16[4,8,256]{2,0,1:T(4,128)(2,1)}), bf16[4,8,256]{2,0,1:T(4,128)(2,1)S(1)}, u32[]{:S(2)}, u32[]{:S(2)}) async-start(bf16[4,8,256]{2,0,1:T(4,128)(2,1)} %bitcast), calls=%async_computation | async-start | bytes 32768 | tf_op jit(solution)/shard_map/all_to_all | solution.py:37
  16.8 103.5 %reduce-scatter.2.cloned.1.call-start = ((), (), s32[]{:S(2)}) async-start(), calls=%async_computation.5 | async-start | bytes 40960 | tf_op jit(solution)/shard_map/reduce_scatter | solution.py:99
  82.1 8.8 %copy-start.4 = (bf16[4,2048]{1,0:T(4,128)(2,1)S(1)}, bf16[4,2048]{1,0:T(4,128)(2,1)}, u32[]{:S(2)}) copy-start(bf16[4,2048]{1,0:T(4,128)(2,1)} %param.15) | copy-start | bytes 49156
  82.1 9.0 %copy-start.6 = (f32[2048]{0:T(1024)S(1)}, f32[2048]{0:T(1024)}, u32[]{:S(2)}) copy-start(f32[2048]{0:T(1024)} %param.23) | copy-start | bytes 24580
  83.2 18.4 %copy-start.1 = (bf16[1,2048,192]{1,2,0:T(8,128)(2,1)S(1)}, bf16[1,2048,192]{1,2,0:T(8,128)(2,1)}, u32[]{:S(2)}) copy-start(bf16[1,2048,192]{1,2,0:T(8,128)(2,1)} %param.27) | copy-start | bytes 2359300
  83.6 18.4 %copy-start.2 = (bf16[1,192,2048]{2,1,0:T(8,128)(2,1)S(1)}, bf16[1,192,2048]{2,1,0:T(8,128)(2,1)}, u32[]{:S(2)}) copy-start(bf16[1,192,2048]{2,1,0:T(8,128)(2,1)} %param.29) | copy-start | bytes 2359300
  83.6 18.4 %copy-start.3 = (bf16[1,2048,192]{1,2,0:T(8,128)(2,1)S(1)}, bf16[1,2048,192]{1,2,0:T(8,128)(2,1)}, u32[]{:S(2)}) copy-start(bf16[1,2048,192]{1,2,0:T(8,128)(2,1)} %param.28) | copy-start | bytes 2359300
  83.6 19.7 %copy-start.7 = (bf16[4,2]{0,1:T(2,128)(2,1)S(1)}, bf16[4,2]{0,1:T(2,128)(2,1)}, u32[]{:S(2)}) copy-start(bf16[4,2]{0,1:T(2,128)(2,1)} %param.26) | copy-start | bytes 52
  122.3 12.0 %all-to-all-start.2 = ((bf16[8,2,256]{2,1,0:T(2,128)(2,1)}), bf16[8,2,256]{2,1,0:T(2,128)(2,1)S(1)}, u32[]{:S(2)}, u32[]{:S(2)}) async-start(bf16[8,2,256]{2,1,0:T(2,128)(2,1)} %reshape.169), calls=%async_computation.3 | async-start | bytes 16384 | tf_op jit(solution)/shard_map/all_to_all | solution.py:102
Sparse Core Ops, SparseCore 0:
  9.4 53.7 all-gather.3
  103.4 16.8 reduce-scatter.1
